TPU v7x, 32 devices: a whole 2x2x4 slice. The times are simulated.
32 devices in a mesh: ep: 16 (over z, y, x), tp: 2 (over core).
Axes of the slice: x: 2, y: 2, z: 4, core: 2. Of those that a mesh axis runs over, the one named last changes fastest.
Arguments:
- tokens: bfloat16 [2048, 2048], P('ep', 'tp'), may hold values from -6 to 6
- cotangent: bfloat16 [2048, 2048], P('ep', 'tp'), may hold values from -6 to 6
- routes: int32 [2048, 2], P('ep'), may hold values from 0 to 15, all different within a row; in each aligned block of 128 rows (0 to 127, 128 to 255, ...) at most 24 rows name the same one
- route_weights: float32 [2048, 2], P('ep'), may hold values from 0.1 to 2.5
- gate_proj: bfloat16 [16, 2048, 512], P('ep', None, 'tp'), may hold values from -0.125 to 0.125
- up_proj: bfloat16 [16, 2048, 512], P('ep', None, 'tp'), may hold values from -0.125 to 0.125
- down_proj: bfloat16 [16, 512, 2048], P('ep', 'tp'), may hold values from -0.25 to 0.25
- shared_gate: bfloat16 [2048, 512], P(None, 'tp'), may hold values from -0.125 to 0.125
- shared_up: bfloat16 [2048, 512], P(None, 'tp'), may hold values from -0.125 to 0.125
- shared_down: bfloat16 [2048, 512], P(None, 'tp'), may hold values from -0.25 to 0.25
Outputs:
- token_grad: bfloat16 [2048, 2048], P('ep', 'tp')
- weight_grad: float32 [2048, 2], P('ep')
- gate_grad: bfloat16 [16, 2048, 512], P('ep', None, 'tp')
- up_grad: bfloat16 [16, 2048, 512], P('ep', None, 'tp')
- down_grad: bfloat16 [16, 512, 2048], P('ep', 'tp')
- sharedgate_grad: float32 [2048, 512], P('ep', 'tp')
- sharedup_grad: float32 [2048, 512], P('ep', 'tp')
- shareddown_grad: float32 [2048, 512], P('ep', 'tp')
Inputs may be any that keep to these rules, and one draw needn't show every extreme that they name: `routes`: the 2 entries of a token name different experts. Among the 128 tokens of one group no expert is named more than 24 times, and in some groups an expert is named exactly 24 times.
All inputs are finite; a program needn't handle non-finite values.
Results may differ from a plain program's by a relative error of at most 0.007.
Values may be sent and summed in bfloat16 or wider, within the bound.
A program may use at most 128 MiB of HBM per device.

v0:
```python
import jax
import jax.numpy as jnp
from jax import lax
from jax.sharding import PartitionSpec as P


def slot_table(routes, experts, capacity):
    assigned = routes.shape[0] * routes.shape[1]
    flat_routes = routes.reshape(assigned)
    onehot = (flat_routes[:, None] == jnp.arange(experts, dtype=jnp.int32)[None, :]).astype(
        jnp.int32
    )
    before = jnp.cumsum(onehot, axis=0) - onehot
    slot_rank = jnp.sum(before * onehot, axis=1)
    slot_of = flat_routes * capacity + slot_rank
    empty = jnp.full((experts * capacity,), assigned, jnp.int32)
    slot_owner = empty.at[slot_of].set(jnp.arange(assigned, dtype=jnp.int32))
    return (slot_of, slot_owner)


def silu_parts(preact):
    sigmoid_v = jax.nn.sigmoid(preact)
    return (preact * sigmoid_v, sigmoid_v * (1.0 + preact * (1.0 - sigmoid_v)))


def rounded(partial_value):
    return lax.optimization_barrier(partial_value.astype(jnp.bfloat16)).astype(jnp.float32)


def contract_rows(left, right):
    return lax.dot_general(
        left, right, (((0,), (0,)), ((), ())), preferred_element_type=jnp.float32
    )


def contract_cols(left, right):
    return lax.dot_general(
        left, right, (((1,), (1,)), ((), ())), preferred_element_type=jnp.float32
    )


def per_device(
    tokens,
    cotangent,
    routes,
    route_weights,
    gate_proj,
    up_proj,
    down_proj,
    shared_gate,
    shared_up,
    shared_down,
):
    groups = lax.axis_size("ep")
    halves = lax.axis_size("tp")
    local_count = gate_proj.shape[0]
    experts = groups * local_count
    token_rows, top = routes.shape
    assigned = token_rows * top
    capacity = assigned // experts + assigned // (2 * experts)
    per_peer = local_count * capacity
    whole_rows, whole_cot = (
        lax.all_gather(tokens, "tp", axis=1, tiled=True),
        lax.all_gather(cotangent, "tp", axis=1, tiled=True),
    )
    slot_of, slot_owner = slot_table(routes, experts, capacity)
    filled = slot_owner < assigned
    owner_safe = jnp.minimum(slot_owner, assigned - 1)
    slot_token = owner_safe // top
    slot_weight = jnp.where(
        filled, route_weights.reshape(assigned)[owner_safe], jnp.zeros((), jnp.float32)
    )
    col_count = tokens.shape[1]
    packed_rows = jnp.where(filled[:, None], tokens[slot_token], jnp.zeros((), jnp.bfloat16))
    packed_cot = (slot_weight[:, None] * cotangent[slot_token].astype(jnp.float32)).astype(
        jnp.bfloat16
    )
    sent_rows = packed_rows.reshape(groups, per_peer, col_count)
    sent_cot = packed_cot.reshape(groups, per_peer, col_count)
    half_rows, half_cot = (
        lax.all_to_all(sent_rows, "ep", split_axis=0, concat_axis=0, tiled=True),
        lax.all_to_all(sent_cot, "ep", split_axis=0, concat_axis=0, tiled=True),
    )
    got_rows, got_cot = (
        lax.all_gather(half_rows, "tp", axis=2, tiled=True),
        lax.all_gather(half_cot, "tp", axis=2, tiled=True),
    )

    def by_expert(layout):
        return jnp.swapaxes(layout.reshape(groups, local_count, capacity, -1), 0, 1).reshape(
            local_count, groups * capacity, -1
        )

    def by_peer(layout):
        return jnp.swapaxes(layout.reshape(local_count, groups, capacity, -1), 0, 1).reshape(
            groups * per_peer, -1
        )

    slot_rows = by_expert(got_rows)
    slot_cot = by_expert(got_cot)
    gate_pre = jnp.einsum("erd,edf->erf", slot_rows, gate_proj, preferred_element_type=jnp.float32)
    up_pre = jnp.einsum("erd,edf->erf", slot_rows, up_proj, preferred_element_type=jnp.float32)
    gate_act, gate_slope = silu_parts(gate_pre)
    hidden = gate_act * up_pre
    back_grad = jnp.einsum("erd,efd->erf", slot_cot, down_proj, preferred_element_type=jnp.float32)
    product = jnp.sum(hidden * back_grad, axis=2, keepdims=True)
    hidden_low = hidden.astype(jnp.bfloat16)
    down_grad = jnp.einsum(
        "erf,erd->efd", hidden_low, slot_cot, preferred_element_type=jnp.float32
    ).astype(jnp.bfloat16)
    gate_delta = (back_grad * up_pre * gate_slope).astype(jnp.bfloat16)
    up_delta = (back_grad * gate_act).astype(jnp.bfloat16)
    gate_grad = jnp.einsum(
        "erd,erf->edf", slot_rows, gate_delta, preferred_element_type=jnp.float32
    ).astype(jnp.bfloat16)
    up_grad = jnp.einsum(
        "erd,erf->edf", slot_rows, up_delta, preferred_element_type=jnp.float32
    ).astype(jnp.bfloat16)
    input_part = jnp.einsum(
        "erf,edf->erd", gate_delta, gate_proj, preferred_element_type=jnp.float32
    )
    input_part = input_part + jnp.einsum(
        "erf,edf->erd", up_delta, up_proj, preferred_element_type=jnp.float32
    )
    mix_gate = jnp.dot(whole_rows, shared_gate, preferred_element_type=jnp.float32)
    mix_up = jnp.dot(whole_rows, shared_up, preferred_element_type=jnp.float32)
    mix_act, mix_slope = silu_parts(mix_gate)
    mix_hidden = (mix_act * mix_up).astype(jnp.bfloat16)
    mix_back = jnp.dot(whole_cot, shared_down, preferred_element_type=jnp.float32)
    mixgrad_gate = (mix_back * mix_up * mix_slope).astype(jnp.bfloat16)
    mixgrad_up = (mix_back * mix_act).astype(jnp.bfloat16)
    mix_partial = contract_cols(mixgrad_gate, shared_gate) + contract_cols(mixgrad_up, shared_up)
    product_cols = jnp.broadcast_to(by_peer(product), (groups * per_peer, halves))
    slot_sum, mix_sum, product_sum = (
        lax.psum_scatter(
            rounded(by_peer(input_part)).astype(jnp.bfloat16), "tp", scatter_dimension=1, tiled=True
        ).astype(jnp.float32),
        lax.psum_scatter(
            rounded(mix_partial).astype(jnp.bfloat16), "tp", scatter_dimension=1, tiled=True
        ).astype(jnp.float32),
        lax.psum_scatter(
            rounded(product_cols).astype(jnp.bfloat16), "tp", scatter_dimension=1, tiled=True
        ).astype(jnp.float32),
    )
    back_rows = slot_sum.astype(jnp.bfloat16).reshape(groups, per_peer, -1)
    back_prod = product_sum.astype(jnp.bfloat16).reshape(groups, per_peer)
    home_rows, home_prod = (
        lax.all_to_all(back_rows, "ep", split_axis=0, concat_axis=0, tiled=True),
        lax.all_to_all(back_prod, "ep", split_axis=0, concat_axis=0, tiled=True),
    )
    per_slot = home_rows.reshape(experts * capacity, -1)[slot_of].astype(jnp.float32)
    token_grad = (mix_sum + jnp.sum(per_slot.reshape(token_rows, top, -1), axis=1)).astype(
        jnp.bfloat16
    )
    slot_product = home_prod.reshape(experts * capacity)[slot_of].astype(jnp.float32)
    weight_grad = slot_product.reshape(token_rows, top) / route_weights
    mix_cols = mixgrad_gate.shape[1]
    stacked = lax.psum_scatter(
        jnp.concatenate(
            [
                contract_rows(whole_rows, mixgrad_gate),
                contract_rows(whole_rows, mixgrad_up),
                contract_rows(whole_cot, mix_hidden),
            ],
            axis=1,
        ),
        "ep",
        scatter_dimension=0,
        tiled=True,
    )
    return (
        token_grad,
        weight_grad,
        gate_grad,
        up_grad,
        down_grad,
        stacked[:, :mix_cols],
        stacked[:, mix_cols : 2 * mix_cols],
        stacked[:, 2 * mix_cols :],
    )


def solution(mesh):
    in_specs = (
        P("ep", "tp"),
        P("ep", "tp"),
        P("ep", None),
        P("ep", None),
        P("ep", None, "tp"),
        P("ep", None, "tp"),
        P("ep", "tp", None),
        P(None, "tp"),
        P(None, "tp"),
        P(None, "tp"),
    )
    out_specs = (
        P("ep", "tp"),
        P("ep", None),
        P("ep", None, "tp"),
        P("ep", None, "tp"),
        P("ep", "tp", None),
        P("ep", "tp"),
        P("ep", "tp"),
        P("ep", "tp"),
    )
    return jax.shard_map(
        per_device, mesh=mesh, in_specs=in_specs, out_specs=out_specs, check_vma=False
    )
```

profile of v0, /device:TPU:12, one launch (start us, length us, event | category | flops | bytes accessed | tf_op | source)
XLA Modules:
  0.0 280.8 jit_solution(13008008762997637790)
XLA Ops:
  12.6 2.8 gather_fusion
  15.5 2.1 gather_fusion.2
  18.6 7.2 %all-to-all-start.1 = ((bf16[16,24,1024]{2,1,0:T(8,128)(2,1)}), bf16[16,24,1024]{2,1,0:T(8,128)(2,1)S(1)}, u32[]{:S(2)}, u32[]{:S(2)}) async-start(bf16[16,24,1024]{2,1,0:T(8,128)(2,1)} %broadcast_select_fusion), calls=%async_computation.2 | async-start | bytes 1572864 | tf_op jit(solution)/shard_map/all_to_all | solution.py:81
  25.9 2.1 gather_fusion.1
  28.0 17.4 %all-to-all-done.1 = bf16[16,24,1024]{2,1,0:T(8,128)(2,1)S(1)} async-done(((bf16[16,24,1024]{2,1,0:T(8,128)(2,1)}), bf16[16,24,1024]{2,1,0:T(8,128)(2,1)S(1)}, u32[]{:S(2)}, u32[]{:S(2)}) %all-to-all-start.1) | async-done | bytes 786464 | tf_op jit(solution)/shard_map/all_to_all | solution.py:81
  46.5 23.5 %all_to_all.25 = bf16[16,24,1024]{2,1,0:T(8,128)(2,1)} all-to-all(bf16[16,24,1024]{2,1,0:T(8,128)(2,1)S(1)} %fusion.4), channel_id=1, replica_groups=mesh['ep'=16,'tp'=2] {'ep'}, dimensions={0} | all-to-all | bytes 1572864 | tf_op jit(solution)/shard_map/all_to_all | solution.py:82
  70.1 3.3 %fusion.10 = f32[384,256]{0,1:T(8,128)} fusion(bf16[384,2048]{1,0:T(8,128)(2,1)} %bitcast.82, bf16[1,2048,256]{2,1,0:T(8,128)(2,1)} %param.15), kind=kOutput, calls=%fused_computation.26 | convolution fusion | flops 402653184 | bytes 3014656 | tf_op jit(solution)/shard_map/erd,edf->erf/dot_general | solution.py:102
  75.0 4.3 %all-gather.3.cloned.1.call-done = bf16[16,24,2048]{2,1,0:T(8,128)(2,1)} async-done(((bf16[16,24,1024]{2,1,0:T(8,128)(2,1)}), bf16[16,24,2048]{2,1,0:T(8,128)(2,1)}) %all-gather.3.cloned.1.call-update) | async-done | bytes 1572880 | tf_op jit(solution)/shard_map/all_gather | solution.py:86
  79.3 2.7 multiply_reduce_fusion
  83.9 1.9 add_convert_fusion
  85.9 2.3 all_gather.13
  88.2 2.2 all_gather.12
  90.4 1.8 fusion.30
  98.4 3.1 %pad_maximum_fusion = f32[2048,768]{0,1:T(8,128)} fusion(f32[2048,256]{0,1:T(8,128)S(1)} %convolution_bitcast_fusion, f32[2048,256]{0,1:T(8,128)S(1)} %convolution_bitcast_fusion.1, f32[2048,256]{0,1:T(8,128)S(1)} %convolution_bitcast_fusion.2), kind=kLoop, calls=%fused_computation.6 | loop fusion | flops 3145728 | bytes 12582912 | tf_op jit(solution)/shard_map/concatenate | solution.py:159
  102.7 2.4 all-reduce
  105.9 11.8 %all_to_all.26 = bf16[16,1,24]{2,1,0:T(2,128)(2,1)S(1)} all-to-all(bf16[16,1,24]{2,1,0:T(2,128)(2,1)S(1)} %all_to_all.20), channel_id=1, replica_groups=mesh['ep'=16,'tp'=2] {'ep'}, dimensions={0} | all-to-all | bytes 1536 | tf_op jit(solution)/shard_map/all_to_all | solution.py:149
  117.8 5.8 %all-to-all-start.2 = ((bf16[16,24,1024]{2,1,0:T(8,128)(2,1)}), bf16[16,24,1024]{2,1,0:T(8,128)(2,1)S(1)}, u32[]{:S(2)}, u32[]{:S(2)}) async-start(bf16[16,24,1024]{2,1,0:T(8,128)(2,1)} %bitcast.88), calls=%async_computation.4 | async-start | bytes 1572864 | tf_op jit(solution)/shard_map/all_to_all | solution.py:148
  123.6 2.7 fusion
  126.3 1.7 fusion.1
  128.0 1.7 fusion.2
  129.8 1.9 gather_fusion.4
  132.6 27.1 %all-to-all-done.2 = bf16[16,24,1024]{2,1,0:T(8,128)(2,1)S(1)} async-done(((bf16[16,24,1024]{2,1,0:T(8,128)(2,1)}), bf16[16,24,1024]{2,1,0:T(8,128)(2,1)S(1)}, u32[]{:S(2)}, u32[]{:S(2)}) %all-to-all-start.2) | async-done | bytes 786464 | tf_op jit(solution)/shard_map/all_to_all | solution.py:148
  162.8 1.7 add_convert_fusion.1
  164.5 106.4 %reduce-scatter.8.cloned.1.call-done = f32[128,768]{0,1:T(8,128)} async-done(((f32[2048,768]{0,1:T(8,128)}), f32[128,768]{0,1:T(8,128)}) %reduce-scatter.8.cloned.1.call-update) | async-done | bytes 393232 | tf_op jit(solution)/shard_map/reduce_scatter | solution.py:158
  (105 shorter events, 26.7 us)
Async XLA Ops:
  7.2 66.3 %copy-start = (bf16[1,2048,256]{2,1,0:T(8,128)(2,1)S(1)}, bf16[1,2048,256]{2,1,0:T(8,128)(2,1)}, u32[]{:S(2)}) copy-start(bf16[1,2048,256]{2,1,0:T(8,128)(2,1)} %param.14) | copy-start | bytes 3145732
  7.2 8.3 %copy-start.1 = (bf16[128,1024]{1,0:T(8,128)(2,1)S(1)}, bf16[128,1024]{1,0:T(8,128)(2,1)}, u32[]{:S(2)}) copy-start(bf16[128,1024]{1,0:T(8,128)(2,1)} %param.10) | copy-start | bytes 786436
  17.6 8.3 %copy-start.2 = (bf16[128,1024]{1,0:T(8,128)(2,1)S(1)}, bf16[128,1024]{1,0:T(8,128)(2,1)}, u32[]{:S(2)}) copy-start(bf16[128,1024]{1,0:T(8,128)(2,1)} %param.11) | copy-start | bytes 786436
  18.6 26.8 %all-to-all-start.1 = ((bf16[16,24,1024]{2,1,0:T(8,128)(2,1)}), bf16[16,24,1024]{2,1,0:T(8,128)(2,1)S(1)}, u32[]{:S(2)}, u32[]{:S(2)}) async-start(bf16[16,24,1024]{2,1,0:T(8,128)(2,1)} %broadcast_select_fusion), calls=%async_computation.2 | async-start | bytes 1572864 | tf_op jit(solution)/shard_map/all_to_all | solution.py:81
  25.8 44.3 %all-gather.5.cloned.1.call-start = ((), (), s32[]{:S(2)}) async-start(), calls=%async_computation.9 | async-start | bytes 2359296 | tf_op jit(solution)/shard_map/all_gather | solution.py:85
  46.3 33.0 %all-gather.3.cloned.1.call-start = ((), (), s32[]{:S(2)}) async-start(), calls=%async_computation.8 | async-start | bytes 2359296 | tf_op jit(solution)/shard_map/all_gather | solution.py:86
  70.0 47.7 %reduce-scatter.6.cloned.1.call-start = ((), (), s32[]{:S(2)}) async-start(), calls=%async_computation.10 | async-start | bytes 2359296 | tf_op jit(solution)/shard_map/reduce_scatter | solution.py:135
  70.1 3.3 %copy-start.3 = (bf16[16,24,2048]{2,1,0:T(8,128)(2,1)S(1)}, bf16[16,24,2048]{2,1,0:T(8,128)(2,1)}, u32[]{:S(2)}) copy-start(bf16[16,24,2048]{2,1,0:T(8,128)(2,1)} %all-gather.5.cloned.1.call-done) | copy-start | bytes 4718596
  82.0 1.3 copy-start.12
  82.7 1.2 copy-start.6
  85.8 77.0 %reduce-scatter.4.cloned.1.call-start = ((), (), s32[]{:S(2)}) async-start(), calls=%async_computation.7 | async-start | bytes 786432 | tf_op jit(solution)/shard_map/reduce_scatter | solution.py:138
  85.9 6.3 %copy-start.7 = (bf16[2048,256]{1,0:T(8,128)(2,1)S(1)}, bf16[2048,256]{1,0:T(8,128)(2,1)}, u32[]{:S(2)}) copy-start(bf16[2048,256]{1,0:T(8,128)(2,1)} %param.17) | copy-start | bytes 3145732
  88.2 4.3 %copy-start.4 = (bf16[128,2048]{1,0:T(8,128)(2,1)}, bf16[128,2048]{1,0:T(8,128)(2,1)S(1)}, u32[]{:S(2)}) copy-start(bf16[128,2048]{1,0:T(8,128)(2,1)S(1)} %all_gather.13) | copy-start | bytes 1572868
  90.4 2.1 copy-start.10
  90.4 2.1 copy-start.19
  92.9 1.3 copy-start.8
  94.2 1.4 copy-start.5
  95.5 175.4 %reduce-scatter.8.cloned.1.call-start = ((), (), s32[]{:S(2)}) async-start(), calls=%async_computation.11 | async-start | bytes 6684672 | tf_op jit(solution)/shard_map/reduce_scatter | solution.py:158
  96.9 1.0 copy-start.11
  117.8 41.9 %all-to-all-start.2 = ((bf16[16,24,1024]{2,1,0:T(8,128)(2,1)}), bf16[16,24,1024]{2,1,0:T(8,128)(2,1)S(1)}, u32[]{:S(2)}, u32[]{:S(2)}) async-start(bf16[16,24,1024]{2,1,0:T(8,128)(2,1)} %bitcast.88), calls=%async_computation.4 | async-start | bytes 1572864 | tf_op jit(solution)/shard_map/all_to_all | solution.py:148
  123.5 2.7 copy-start.13
  126.3 1.7 copy-start.15
  126.3 1.7 copy-start.16
  126.3 1.7 copy-start.18
  (4 other events, 2.8 us)
Sparse Core Ops, SparseCore 0:
  46.4 9.0 all-gather.4
  70.2 9.1 all-gather.2
  86.0 10.2 reduce-scatter.5
  98.4 9.0 reduce-scatter.3
  112.5 158.4 reduce-scatter.7
where the time goes:
time: 284 us; the launch traced here: 281 us
  waiting for transfers between devices  155 us (55%)
  blocking collectives  42.2 us (15%)
  local copies, waits for them, and re-layouts  24.6 us (9%)
  matrix products  22.6 us (8%)
  between operations  14.2 us (5%)
  starting transfers between devices  13.1 us (5%)
  other arithmetic  8.74 us (3%)
    reduce_scatter x1, waiting for transfers between devices, per_device(): lax.psum_scatter(jnp.concatenate([contract_rows(whole_rows, mixgrad_gate)...  106 us
    all_to_all x1, waiting for transfers between devices, per_device(): lax.all_to_all(back_rows, 'ep', split_axis=0, concat_axis=0, tiled=True)  27.1 us
    all_to_all x1, blocking collectives, per_device(): lax.all_to_all(sent_cot, 'ep', split_axis=0, concat_axis=0, tiled=True)  23.5 us
    all_to_all x1, waiting for transfers between devices, per_device(): lax.all_to_all(sent_rows, 'ep', split_axis=0, concat_axis=0, tiled=True)  17.4 us
    all_to_all x1, blocking collectives, per_device(): lax.all_to_all(back_prod, 'ep', split_axis=0, concat_axis=0, tiled=True)  11.8 us
    unnamed x50, local copies, waits for them, and re-layouts  10.1 us
    all_to_all x1, starting transfers between devices, per_device(): lax.all_to_all(sent_rows, 'ep', split_axis=0, concat_axis=0, tiled=True)  7.17 us
    all_to_all x1, starting transfers between devices, per_device(): lax.all_to_all(back_rows, 'ep', split_axis=0, concat_axis=0, tiled=True)  5.78 us
  transfers between devices with their start and end apart: 7, of which 4 were waited for; matrix products, arithmetic and copies ran while one was open for 11% of the time, Pallas kernels for 0%

commit v1 on v0

v1 whole, which is shorter than its diff:
```python
import functools

import jax
import jax.numpy as jnp
from jax import lax
from jax.experimental import pallas as pl
from jax.experimental.pallas import tpu as pltpu
from jax.sharding import PartitionSpec as P

MESH = pl.DeviceIdType.MESH
F32 = jnp.float32
BF16 = jnp.bfloat16


def remote(src, dst, send, recv, device):
    return pltpu.make_async_remote_copy(
        src_ref=src,
        dst_ref=dst,
        send_sem=send,
        recv_sem=recv,
        device_id=device,
        device_id_type=MESH,
    )


def silu_parts(preact):
    sigmoid_v = jax.nn.sigmoid(preact)
    return (preact * sigmoid_v, sigmoid_v * (1.0 + preact * (1.0 - sigmoid_v)))


def dot_nn(left, right):
    return lax.dot_general(left, right, (((1,), (0,)), ((), ())), preferred_element_type=F32)


def dot_nt(left, right):
    return lax.dot_general(left, right, (((1,), (1,)), ((), ())), preferred_element_type=F32)


def dot_tn(left, right):
    return lax.dot_general(left, right, (((0,), (0,)), ((), ())), preferred_element_type=F32)


def loop(first, last, body):
    def step(s, carry):
        body(s)
        return carry

    lax.fori_loop(first, last, step, 0)


def greet(groups, me, half):
    barrier = pltpu.get_barrier_semaphore()

    def hello(s):
        pl.semaphore_signal(
            barrier, inc=1, device_id=(lax.rem(me + s, groups), half), device_id_type=MESH
        )

    loop(1, groups, hello)
    pl.semaphore_signal(barrier, inc=1, device_id=(me, 1 - half), device_id_type=MESH)
    pl.semaphore_wait(barrier, groups)


def dispatch_kernel(
    groups,
    inner,
    both,
    packed,
    cut,
    sgate,
    sup,
    sdown,
    got,
    mix_out,
    grad_gate,
    grad_up,
    grad_down,
    whole,
    cut_all,
    mixed,
    mix_part,
    mix_in,
    part,
    part_in,
    pair_sem,
    mixp_sem,
    own_sem,
    out_sem,
    in_sem,
    fwd_out_sem,
    fwd_in_sem,
    cut_sem,
    mixed_sem,
    part_sem,
):
    me = lax.axis_index("ep")
    half = lax.axis_index("tp")
    other = 1 - half
    outer = groups // inner
    slow = me // inner
    fast = me % inner
    cols = both.shape[2]
    hid = sgate.shape[1]
    cut_cols = cut.shape[3]
    mine = pl.ds(pl.multiple_of(half * cols, cols), cols)
    theirs = pl.ds(pl.multiple_of(other * cols, cols), cols)
    cut_mine = pl.ds(pl.multiple_of(half * cut_cols, cut_cols), cut_cols)
    cut_theirs = pl.ds(pl.multiple_of(other * cut_cols, cut_cols), cut_cols)
    partner = (me, other)

    greet(groups, me, half)

    pair = remote(both, whole.at[:, :, mine], pair_sem.at[0], pair_sem.at[1], partner)
    pair.start()
    own_whole = pltpu.make_async_copy(both, whole.at[:, :, mine], own_sem.at[0])
    own_whole.start()

    def member(step):
        to = (fast + step) % inner
        return to, (slow * inner + to, half)

    def source(step):
        return (fast + inner - step) % inner

    for step in range(1, inner):
        to, device = member(step)
        remote(
            cut.at[:, to],
            cut_all.at[:, fast, :, cut_mine],
            cut_sem.at[0, to],
            cut_sem.at[1, fast],
            device,
        ).start()
    own_cut = pltpu.make_async_copy(
        cut.at[:, fast], cut_all.at[:, fast, :, cut_mine], own_sem.at[1]
    )
    own_cut.start()
    remote(
        cut.at[:, fast],
        cut_all.at[:, fast, :, cut_mine],
        cut_sem.at[2, fast],
        cut_sem.at[3, fast],
        partner,
    ).start()

    own_slot = pltpu.make_async_copy(packed.at[:, me], got.at[:, me, :, mine], own_sem.at[2])
    own_slot.start()
    remote(
        packed.at[:, me], got.at[:, me, :, mine], fwd_out_sem.at[me], fwd_in_sem.at[me], partner
    ).start()

    def send_slots(s):
        to = lax.rem(me + s, groups)
        remote(
            packed.at[:, to], got.at[:, me, :, mine], out_sem.at[to], in_sem.at[me], (to, half)
        ).start()

    middle = groups // 2
    loop(1, middle, send_slots)

    own_whole.wait()
    remote(both, whole.at[:, :, theirs], pair_sem.at[0], pair_sem.at[1], partner).wait()

    rows = whole[0]
    mix_gate = dot_nn(rows, sgate[...])
    mix_up = dot_nn(rows, sup[...])
    mix_back = dot_nn(whole[1], sdown[...])
    act, slope = silu_parts(mix_gate)
    low_gate = (mix_back * mix_up * slope).astype(BF16)
    low_up = (mix_back * act).astype(BF16)
    mixed[fast, :, 0:hid] = low_gate
    mixed[fast, :, hid : 2 * hid] = low_up
    mixed[fast, :, 2 * hid : 3 * hid] = (act * mix_up).astype(BF16)

    for step in range(1, inner):
        to, device = member(step)
        remote(
            mixed.at[fast], mixed.at[fast], mixed_sem.at[0, to], mixed_sem.at[1, fast], device
        ).start()

    loop(middle, groups, send_slots)

    for piece in range(2):
        at = pl.ds(piece * cols, cols)
        mix_part[piece] = (
            dot_nt(low_gate, sgate[at, :]) + dot_nt(low_up, sup[at, :])
        ).astype(BF16)
    mixp = remote(mix_part.at[other], mix_in, mixp_sem.at[0], mixp_sem.at[1], partner)
    mixp.start()

    own_cut.wait()
    for step in range(1, inner):
        frm = source(step)
        here = cut_all.at[:, frm, :, cut_mine]
        remote(
            cut.at[:, frm], here, cut_sem.at[0, frm], cut_sem.at[1, frm], partner
        ).wait_recv()
        remote(here, here, cut_sem.at[2, frm], cut_sem.at[3, frm], partner).start()

    mixp.wait()
    mix_out[...] = mix_part[half].astype(F32) + mix_in[...].astype(F32)

    for step in range(inner):
        frm = source(step)
        here = cut_all.at[:, frm, :, cut_mine]
        there = cut_all.at[:, frm, :, cut_theirs]
        remote(here, there, cut_sem.at[2, frm], cut_sem.at[3, frm], partner).wait()
        if step > 0:
            to, device = member(step)
            remote(
                cut.at[:, to], here, cut_sem.at[0, to], cut_sem.at[1, to], device
            ).wait_send()
            remote(
                mixed.at[fast], mixed.at[frm], mixed_sem.at[0, to], mixed_sem.at[1, frm], device
            ).wait()

    depth = inner * cut.shape[2]
    wide = 2 * cut_cols
    every = mixed[...].reshape(depth, 3 * hid)
    block = part.shape[1]
    part[:, :, 0 : 2 * hid] = (
        dot_tn(cut_all[0].reshape(depth, wide), every[:, 0 : 2 * hid])
        .astype(BF16)
        .reshape(outer, block, 2 * hid)
    )
    part[:, :, 2 * hid : 3 * hid] = (
        dot_tn(cut_all[1].reshape(depth, wide), every[:, 2 * hid : 3 * hid])
        .astype(BF16)
        .reshape(outer, block, hid)
    )

    def send_part(s):
        to = lax.rem(slow + s, outer)
        remote(
            part.at[to],
            part_in.at[slow],
            part_sem.at[0, to],
            part_sem.at[1, slow],
            (to * inner + fast, half),
        ).start()

    loop(1, outer, send_part)

    def forward(s):
        frm = lax.rem(me + groups - s, groups)
        here = got.at[:, frm, :, mine]
        remote(packed.at[:, frm], here, out_sem.at[frm], in_sem.at[frm], partner).wait_recv()
        remote(here, here, fwd_out_sem.at[frm], fwd_in_sem.at[frm], partner).start()

    loop(1, groups, forward)

    total = part[slow].astype(F32)
    grad_gate[...] = total[:, 0:hid]
    grad_up[...] = total[:, hid : 2 * hid]
    grad_down[...] = total[:, 2 * hid : 3 * hid]

    def take_part(s):
        frm = lax.rem(slow + outer - s, outer)
        remote(
            part.at[frm], part_in.at[frm], part_sem.at[0, frm], part_sem.at[1, frm], partner
        ).wait()
        term = part_in[frm].astype(F32)
        grad_gate[...] += term[:, 0:hid]
        grad_up[...] += term[:, hid : 2 * hid]
        grad_down[...] += term[:, 2 * hid : 3 * hid]

    loop(1, outer, take_part)

    own_slot.wait()

    def finish(s):
        frm = lax.rem(me + groups - s, groups)
        here = got.at[:, frm, :, mine]
        there = got.at[:, frm, :, theirs]
        remote(here, there, fwd_out_sem.at[frm], fwd_in_sem.at[frm], partner).wait()

    loop(0, groups, finish)

    def sent(s):
        to = lax.rem(me + s, groups)
        here = got.at[:, to, :, mine]
        remote(packed.at[:, to], here, out_sem.at[to], in_sem.at[to], partner).wait_send()

    loop(1, groups, sent)


def dispatch(groups, inner, both, packed, cut, sgate, sup, sdown):
    _, token_rows, cols = both.shape
    per_peer = packed.shape[2]
    width = 2 * cols
    hid = sgate.shape[1]
    outer = groups // inner
    block = width // groups
    vmem = pl.BlockSpec(memory_space=pltpu.VMEM)
    grad = jax.ShapeDtypeStruct((block, hid), F32)
    dma = pltpu.SemaphoreType.DMA
    return pl.pallas_call(
        functools.partial(dispatch_kernel, groups, inner),
        out_shape=(
            jax.ShapeDtypeStruct((2, groups, per_peer, width), BF16),
            jax.ShapeDtypeStruct((token_rows, cols), F32),
            grad,
            grad,
            grad,
        ),
        in_specs=[vmem] * 6,
        out_specs=(pl.BlockSpec(memory_space=pl.ANY), vmem, vmem, vmem, vmem),
        scratch_shapes=[
            pltpu.VMEM((2, token_rows, width), BF16),
            pltpu.VMEM((2, inner, token_rows, width // inner), BF16),
            pltpu.VMEM((inner, token_rows, 3 * hid), BF16),
            pltpu.VMEM((2, token_rows, cols), BF16),
            pltpu.VMEM((token_rows, cols), BF16),
            pltpu.VMEM((outer, block, 3 * hid), BF16),
            pltpu.VMEM((outer, block, 3 * hid), BF16),
            dma((2,)),
            dma((2,)),
            dma((3,)),
            dma((groups,)),
            dma((groups,)),
            dma((groups,)),
            dma((groups,)),
            dma((4, inner)),
            dma((2, inner)),
            dma((2, outer)),
        ],
        compiler_params=pltpu.CompilerParams(collective_id=0, has_side_effects=True),
        name="dispatch",
    )(both, packed, cut, sgate, sup, sdown)


def home_kernel(groups, terms, home, taken, back, pair_sem, own_sem, out_sem, in_sem):
    me = lax.axis_index("ep")
    half = lax.axis_index("tp")
    other = 1 - half
    greet(groups, me, half)
    pair = remote(terms.at[other], taken, pair_sem.at[0], pair_sem.at[1], (me, other))
    pair.start()
    pair.wait()

    def add(s):
        back[s] = (terms[half, s].astype(F32) + taken[s].astype(F32)).astype(BF16)

    loop(0, groups, add)
    own = pltpu.make_async_copy(back.at[me], home.at[me], own_sem)
    own.start()

    def send(s):
        to = lax.rem(me + s, groups)
        remote(back.at[to], home.at[me], out_sem.at[to], in_sem.at[me], (to, half)).start()

    loop(1, groups, send)
    own.wait()

    def take(s):
        frm = lax.rem(me + groups - s, groups)
        remote(back.at[frm], home.at[frm], out_sem.at[frm], in_sem.at[frm], (frm, half)).wait()

    loop(1, groups, take)


def send_home(groups, terms):
    shape = terms.shape[1:]
    vmem = pl.BlockSpec(memory_space=pltpu.VMEM)
    dma = pltpu.SemaphoreType.DMA
    return pl.pallas_call(
        functools.partial(home_kernel, groups),
        out_shape=jax.ShapeDtypeStruct(shape, BF16),
        in_specs=[vmem],
        out_specs=pl.BlockSpec(memory_space=pl.ANY),
        scratch_shapes=[
            pltpu.VMEM(shape, BF16),
            pltpu.VMEM(shape, BF16),
            dma((2,)),
            dma,
            dma((groups,)),
            dma((groups,)),
        ],
        compiler_params=pltpu.CompilerParams(collective_id=1, has_side_effects=True),
        name="home",
    )(terms)


def per_device(
    tokens,
    cotangent,
    routes,
    route_weights,
    gate_proj,
    up_proj,
    down_proj,
    shared_gate,
    shared_up,
    shared_down,
):
    groups = lax.axis_size("ep")
    halves = lax.axis_size("tp")
    local_count = gate_proj.shape[0]
    experts = groups * local_count
    token_rows, top = routes.shape
    assigned = token_rows * top
    capacity = assigned // experts + assigned // (2 * experts)
    per_peer = local_count * capacity
    slots = experts * capacity
    cols = tokens.shape[1]
    inner = 4
    outer = groups // inner
    block = halves * cols // groups

    names = routes.T
    named = (names[:, :, None] == jnp.arange(experts, dtype=jnp.int32)).astype(BF16)
    order = jnp.arange(token_rows, dtype=jnp.int32)
    earlier = (order[None, :] < order[:, None]).astype(BF16)
    before = dot_nn(earlier, named[0] + named[1])
    rank = jnp.sum(before[None] * named.astype(F32), axis=2)
    slot_of = names * capacity + rank.astype(jnp.int32)
    hit = slot_of[:, None, :] == jnp.arange(slots, dtype=jnp.int32)[None, :, None]
    chosen = (hit[0] | hit[1]).astype(BF16)
    slot_weight = jnp.sum(jnp.where(hit, route_weights.T[:, None, :], 0.0), axis=(0, 2))
    packed_rows = dot_nn(chosen, tokens).astype(BF16)
    packed_cot = (slot_weight[:, None] * dot_nn(chosen, cotangent)).astype(BF16)
    packed = jnp.stack([packed_rows, packed_cot]).reshape(2, groups, per_peer, cols)
    both = jnp.stack([tokens, cotangent])
    cut = (
        both.reshape(2, token_rows, outer // halves, inner, block)
        .transpose(0, 3, 1, 2, 4)
        .reshape(2, inner, token_rows, cols // inner)
    )
    got, mix_sum, sharedgate_grad, sharedup_grad, shareddown_grad = dispatch(
        groups, inner, both, packed, cut, shared_gate, shared_up, shared_down
    )

    def by_expert(layout):
        return jnp.swapaxes(layout.reshape(groups, local_count, capacity, -1), 0, 1).reshape(
            local_count, groups * capacity, -1
        )

    def by_peer(layout):
        return jnp.swapaxes(layout.reshape(local_count, groups, capacity, -1), 0, 1).reshape(
            groups, per_peer, -1
        )

    slot_rows = by_expert(got[0])
    slot_cot = by_expert(got[1])
    gate_pre = jnp.einsum("erd,edf->erf", slot_rows, gate_proj, preferred_element_type=F32)
    up_pre = jnp.einsum("erd,edf->erf", slot_rows, up_proj, preferred_element_type=F32)
    gate_act, gate_slope = silu_parts(gate_pre)
    hidden = gate_act * up_pre
    back_grad = jnp.einsum("erd,efd->erf", slot_cot, down_proj, preferred_element_type=F32)
    product = jnp.sum(hidden * back_grad, axis=2, keepdims=True)
    hidden_low = hidden.astype(BF16)
    gate_delta = (back_grad * up_pre * gate_slope).astype(BF16)
    up_delta = (back_grad * gate_act).astype(BF16)
    input_part = jnp.einsum("erf,edf->erd", gate_delta, gate_proj, preferred_element_type=F32)
    input_part = input_part + jnp.einsum(
        "erf,edf->erd", up_delta, up_proj, preferred_element_type=F32
    )
    sent_part = by_peer(input_part.astype(BF16))
    lanes = jnp.broadcast_to(by_peer(product.astype(BF16)), (groups, per_peer, 128))
    terms = jnp.stack(
        [
            jnp.concatenate([sent_part[:, :, h * cols : (h + 1) * cols], lanes], axis=2)
            for h in range(halves)
        ]
    )
    home = send_home(groups, terms).reshape(slots, cols + 128)

    down_grad = jnp.einsum("erf,erd->efd", hidden_low, slot_cot, preferred_element_type=F32)
    gate_grad = jnp.einsum("erd,erf->edf", slot_rows, gate_delta, preferred_element_type=F32)
    up_grad = jnp.einsum("erd,erf->edf", slot_rows, up_delta, preferred_element_type=F32)

    token_grad = (mix_sum + dot_tn(chosen, home[:, :cols])).astype(BF16)
    slot_product = home[:, cols].astype(F32)
    weight_grad = (
        jnp.sum(jnp.where(hit, slot_product[None, :, None], 0.0), axis=1).T / route_weights
    )
    return (
        token_grad,
        weight_grad,
        gate_grad.astype(BF16),
        up_grad.astype(BF16),
        down_grad.astype(BF16),
        sharedgate_grad,
        sharedup_grad,
        shareddown_grad,
    )


def solution(mesh):
    in_specs = (
        P("ep", "tp"),
        P("ep", "tp"),
        P("ep", None),
        P("ep", None),
        P("ep", None, "tp"),
        P("ep", None, "tp"),
        P("ep", "tp", None),
        P(None, "tp"),
        P(None, "tp"),
        P(None, "tp"),
    )
    out_specs = (
        P("ep", "tp"),
        P("ep", None),
        P("ep", None, "tp"),
        P("ep", None, "tp"),
        P("ep", "tp", None),
        P("ep", "tp"),
        P("ep", "tp"),
        P("ep", "tp"),
    )
    return jax.shard_map(
        per_device, mesh=mesh, in_specs=in_specs, out_specs=out_specs, check_vma=False
    )
```

time: 284 us -> 122 us (0.43); the launches traced: 281 us -> 122 us
  waiting for transfers between devices: 155 us -> 0 us
  Pallas kernels: 0 us -> 91 us
  blocking collectives: 42.2 us -> 0 us
  local copies, waits for them, and re-layouts: 24.6 us -> 8.01 us
  between operations: 14.2 us -> 0.88 us
  starting transfers between devices: 13.1 us -> 0 us
  matrix products: 22.6 us -> 13.9 us
    reduce_scatter x3 -> x0, waiting for transfers between devices: 106 us -> none  [the longest x1 106 us: per_device(): lax.psum_scatter(jnp.concatenate([contract_rows(whole_rows, mixgrad_gate)...]
    pallas_call x0 -> x2, Pallas kernels: none -> 91 us  [the longest x1 61.1 us: dispatch(): pl.pallas_call(functools.partial(dispatch_kernel, groups, inner), out_sha...]
    all_to_all x2 -> x0, waiting for transfers between devices: 44.5 us -> none  [the longest x1 27.1 us: per_device(): lax.all_to_all(back_rows, 'ep', split_axis=0, concat_axis=0, tiled=True)]
    all_to_all x2 -> x0, blocking collectives: 35.3 us -> none  [the longest x1 23.5 us: per_device(): lax.all_to_all(sent_cot, 'ep', split_axis=0, concat_axis=0, tiled=True)]
    all_to_all x2 -> x0, starting transfers between devices: 12.9 us -> none  [the longest x1 7.17 us: per_device(): lax.all_to_all(sent_rows, 'ep', split_axis=0, concat_axis=0, tiled=True)]
    gather x5 -> x0, local copies, waits for them, and re-layouts: 10.1 us -> none  [the longest x1 2.81 us: per_device(): route_weights.reshape(assigned)[owner_safe]]
    dot_general x14 -> x10, matrix products: 19.3 us -> 11.6 us  [the longest x3 2.77 us: dot_nn(): lax.dot_general(left, right, (((1,), (0,)), ((), ())), preferred_element_...]
    unnamed x50 -> x24, local copies, waits for them, and re-layouts: 10.1 us -> 2.55 us
  transfers between devices with their start and end apart: 7 -> 0, of which waited for: 4 -> 0; matrix products, arithmetic and copies ran while one was open for 11% -> 0% of each run, Pallas kernels for 0% -> 0%
where the time goes in v1:
time: 122 us
  Pallas kernels  91 us (75%)
  matrix products  13.9 us (11%)
  other arithmetic  8.25 us (7%)
  local copies, waits for them, and re-layouts  8.01 us (7%)
    pallas_call x1, Pallas kernels, dispatch(): pl.pallas_call(functools.partial(dispatch_kernel, groups, inner), out_sha...  61.1 us
    pallas_call x1, Pallas kernels, send_home(): pl.pallas_call(functools.partial(home_kernel, groups), out_shape=jax.Shap...  29.9 us
    dot_general x3, matrix products, dot_nn(): lax.dot_general(left, right, (((1,), (0,)), ((), ())), preferred_element_...  2.77 us
    unnamed x24, local copies, waits for them, and re-layouts  2.55 us

profile of v1, /device:TPU:12, one launch (start us, length us, event | category | flops | bytes accessed | tf_op | source)
XLA Modules:
  0.0 122.0 jit_solution(874454290035176750)
XLA Ops:
  0.6 0.8 fusion.21
  1.6 0.7 multiply_reduce_fusion.1
  2.3 0.7 convert_add_fusion
  3.0 0.8 select_reduce_fusion.1
  3.9 1.3 %multiply_convert_fusion = bf16[384,1024]{1,0:T(8,128)(2,1)S(1)} fusion(bf16[128,1024]{1,0:T(8,128)(2,1)} %param.11, f32[384]{0:T(512)S(1)} %select_reduce_fusion.1, pred[2,384,128]{2,1,0:T(32,128)(4,1)S(1)} %iota_compare_fusion), kind=kOutput, calls=%fused_computation.9 | convolution fusion | flops 101498880 | bytes 1148416 | tf_op jit(solution)/shard_map/dot_general | solution.py:32
  5.2 1.3 %convolution_convert_fusion.3 = bf16[384,1024]{1,0:T(8,128)(2,1)S(1)} fusion(bf16[128,1024]{1,0:T(8,128)(2,1)} %param.10, pred[2,384,128]{2,1,0:T(32,128)(4,1)S(1)} %iota_compare_fusion), kind=kOutput, calls=%fused_computation.10 | convolution fusion | flops 101105664 | bytes 1146880 | tf_op jit(solution)/shard_map/dot_general | solution.py:32
  6.5 1.3 %pad_maximum_fusion.1.packed = bf16[2,16,24,1024]{3,2,1,0:T(8,128)(2,1)} fusion(bf16[1,16,24,1024]{3,2,1,0:T(8,128)(2,1)S(1)} %bitcast.67, bf16[1,16,24,1024]{3,2,1,0:T(8,128)(2,1)S(1)} %bitcast.68), kind=kLoop, calls=%fused_computation.8 | loop fusion | flops 786432 | bytes 3145728 | tf_op jit(solution)/shard_map/stack | solution.py:422
  8.6 0.7 maximum_bitcast_fusion
  9.4 1.1 reshape.125.cut
  10.5 0.8 pad_maximum_fusion.4.both
  11.3 61.1 %dispatch.1 = (bf16[2,16,24,2048]{3,2,1,0:T(8,128)(2,1)}, f32[128,1024]{1,0:T(8,128)}, f32[128,256]{1,0:T(8,128)}, f32[128,256]{1,0:T(8,128)}, f32[128,256]{1,0:T(8,128)}) custom-call(bf16[2,128,1024]{2,1,0:T(8,128)(2,1)} %pad_maximum_fusion.4.both, bf16[2,16,24,1024]{3,2,1,0:T(8,128)(2,1)} %pad_maximum_fusion.1.packed, ...), custom_call_target="tpu_custom_call" | custom-call | tf_op jit(solution)/shard_map/dispatch/pallas_call | solution.py:297
  72.5 2.4 %fusion.29 = (bf16[1,16,24,2048]{3,2,1,0:T(8,128)(2,1)S(1)}, bf16[1,16,24,2048]{3,2,1,0:T(8,128)(2,1)S(1)}) fusion(bf16[2,16,24,2048]{3,2,1,0:T(8,128)(2,1)} %get-tuple-element.14), kind=kLoop, calls=%fused_computation.52 | loop fusion | bytes 6291456 | tf_op jit(solution)/shard_map/slice | solution.py:443
  74.8 0.8 fusion.9
  76.0 0.7 fusion.11
  76.8 1.0 multiply_convert_fusion.2
  77.7 1.7 %fusion.2 = bf16[1,256,2048]{2,1,0:T(8,128)(2,1)} fusion(bf16[384,2048]{1,0:T(8,128)(2,1)S(1)} %bitcast.72, f32[384,256]{0,1:T(8,128)S(1)} %fusion.9, f32[384,256]{0,1:T(8,128)S(1)} %get-tuple-element.27), kind=kOutput, calls=%fused_computation.6 | convolution fusion | flops 403767296 | bytes 3407872 | tf_op jit(solution)/shard_map/erf,erd->efd/dot_general | solution.py:468
  79.5 1.7 %fusion.1 = bf16[1,2048,256]{2,1,0:T(8,128)(2,1)} fusion(bf16[384,2048]{1,0:T(8,128)(2,1)S(1)} %bitcast.62, bf16[384,256]{0,1:T(8,128)(2,1)S(1)} %get-tuple-element.24), kind=kOutput, calls=%fused_computation.5 | convolution fusion | flops 403177472 | bytes 2818048 | tf_op jit(solution)/shard_map/erd,erf->edf/dot_general | solution.py:470
  81.2 1.7 %fusion = bf16[1,2048,256]{2,1,0:T(8,128)(2,1)} fusion(bf16[384,2048]{1,0:T(8,128)(2,1)S(1)} %bitcast.63, bf16[384,256]{0,1:T(8,128)(2,1)S(1)} %get-tuple-element.22), kind=kOutput, calls=%fused_computation.4 | convolution fusion | flops 403177472 | bytes 2818048 | tf_op jit(solution)/shard_map/erd,erf->edf/dot_general | solution.py:469
  83.5 0.7 add_convert_fusion
  84.7 1.4 %pad_maximum_fusion.terms = bf16[2,16,24,1152]{3,2,1,0:T(8,128)(2,1)} fusion(bf16[1,16,24,1152]{3,2,1,0:T(8,128)(2,1)S(1)} %get-tuple-element.26, bf16[1,16,24,1152]{3,2,1,0:T(8,128)(2,1)S(1)} %get-tuple-element.25), kind=kLoop, calls=%fused_computation.7 | loop fusion | flops 884736 | bytes 3538944 | tf_op jit(solution)/shard_map/stack | solution.py:460
  86.1 29.9 %home.1 = bf16[16,24,1152]{2,1,0:T(8,128)(2,1)} custom-call(bf16[2,16,24,1152]{3,2,1,0:T(8,128)(2,1)} %pad_maximum_fusion.terms), custom_call_target="tpu_custom_call" | custom-call | tf_op jit(solution)/shard_map/home/pallas_call | solution.py:366
  116.0 2.3 %fusion.3 = bf16[128,1024]{1,0:T(8,128)(2,1)} fusion(f32[128,1024]{1,0:T(8,128)S(1)} %copy-done.4, bf16[384,1152]{1,0:T(8,128)(2,1)} %bitcast.65, pred[2,384,128]{2,1,0:T(32,128)(4,1)S(1)} %iota_compare_fusion), kind=kOutput, calls=%fused_computation.14 | convolution fusion | flops 100974592 | bytes 1671168 | tf_op jit(solution)/shard_map/dot_general | solution.py:40
  118.3 0.9 slice.47
  120.0 0.7 copy.33
  (37 shorter events, 4.7 us)
Async XLA Ops:
  0.6 76.1 %copy-start = (bf16[1,2048,256]{2,1,0:T(8,128)(2,1)S(1)}, bf16[1,2048,256]{2,1,0:T(8,128)(2,1)}, u32[]{:S(2)}) copy-start(bf16[1,2048,256]{2,1,0:T(8,128)(2,1)} %param.14) | copy-start | bytes 3145732
  6.5 1.3 %copy-start.3 = (bf16[128,1024]{1,0:T(8,128)(2,1)S(1)}, bf16[128,1024]{1,0:T(8,128)(2,1)}, u32[]{:S(2)}) copy-start(bf16[128,1024]{1,0:T(8,128)(2,1)} %param.10) | copy-start | bytes 786436
  6.5 1.7 %copy-start.2 = (bf16[128,1024]{1,0:T(8,128)(2,1)S(1)}, bf16[128,1024]{1,0:T(8,128)(2,1)}, u32[]{:S(2)}) copy-start(bf16[128,1024]{1,0:T(8,128)(2,1)} %param.11) | copy-start | bytes 786436
  72.4 2.4 %copy-start.1 = (bf16[1,2048,256]{2,1,0:T(8,128)(2,1)S(1)}, bf16[1,2048,256]{2,1,0:T(8,128)(2,1)}, u32[]{:S(2)}) copy-start(bf16[1,2048,256]{2,1,0:T(8,128)(2,1)} %param.15) | copy-start | bytes 3145732
  74.8 1.2 %copy-start.9 = (bf16[1,256,2048]{2,1,0:T(8,128)(2,1)S(1)}, bf16[1,256,2048]{2,1,0:T(8,128)(2,1)}, u32[]{:S(2)}) copy-start(bf16[1,256,2048]{2,1,0:T(8,128)(2,1)} %param.16) | copy-start | bytes 3145732
  86.1 29.9 %copy-start.4 = (f32[128,1024]{1,0:T(8,128)S(1)}, f32[128,1024]{1,0:T(8,128)}, u32[]{:S(2)}) copy-start(f32[128,1024]{1,0:T(8,128)} %get-tuple-element.13) | copy-start | bytes 1572868
  116.0 3.5 %copy-start.8 = (f32[128,2]{0,1:T(2,128)S(1)}, f32[128,2]{0,1:T(2,128)}, u32[]{:S(2)}) copy-start(f32[128,2]{0,1:T(2,128)} %param.13) | copy-start | bytes 3076
  116.0 4.1 %copy-start.7 = (f32[128,256]{1,0:T(8,128)S(1)}, f32[128,256]{1,0:T(8,128)}, u32[]{:S(2)}) copy-start(f32[128,256]{1,0:T(8,128)} %get-tuple-element.41) | copy-start | bytes 393220
  116.0 4.7 %copy-start.6 = (f32[128,256]{1,0:T(8,128)S(1)}, f32[128,256]{1,0:T(8,128)}, u32[]{:S(2)}) copy-start(f32[128,256]{1,0:T(8,128)} %get-tuple-element.42) | copy-start | bytes 393220
  116.0 5.4 %copy-start.5 = (f32[128,256]{1,0:T(8,128)S(1)}, f32[128,256]{1,0:T(8,128)}, u32[]{:S(2)}) copy-start(f32[128,256]{1,0:T(8,128)} %get-tuple-element.43) | copy-start | bytes 393220

commit v2 on v1

--- a/solution.py
+++ b/solution.py
@@ -64,18 +64,21 @@
 def dispatch_kernel(
     groups,
     inner,
-    both,
-    packed,
-    cut,
+    tok,
+    cot,
+    packed_rows,
+    packed_cot,
     sgate,
     sup,
     sdown,
-    got,
+    got_rows,
+    got_cot,
     mix_out,
     grad_gate,
     grad_up,
     grad_down,
     whole,
+    cut,
     cut_all,
     mixed,
     mix_part,
@@ -99,7 +102,11 @@
     outer = groups // inner
     slow = me // inner
     fast = me % inner
-    cols = both.shape[2]
+    cols = tok.shape[1]
+    width = 2 * cols
+    block = width // groups
+    packed = (packed_rows, packed_cot)
+    got = (got_rows, got_cot)
     hid = sgate.shape[1]
     cut_cols = cut.shape[3]
     mine = pl.ds(pl.multiple_of(half * cols, cols), cols)
@@ -108,12 +115,26 @@
     cut_theirs = pl.ds(pl.multiple_of(other * cut_cols, cut_cols), cut_cols)
     partner = (me, other)
 
+    for to in range(inner):
+        for piece in range(outer // 2):
+            frm = pl.ds((piece * inner + to) * block, block)
+            at = pl.ds(piece * block, block)
+            cut[0, to, :, at] = tok[:, frm]
+            cut[1, to, :, at] = cot[:, frm]
+
     greet(groups, me, half)
 
-    pair = remote(both, whole.at[:, :, mine], pair_sem.at[0], pair_sem.at[1], partner)
-    pair.start()
-    own_whole = pltpu.make_async_copy(both, whole.at[:, :, mine], own_sem.at[0])
-    own_whole.start()
+    def own_whole(i):
+        return pltpu.make_async_copy((tok, cot)[i], whole.at[i, :, mine], own_sem.at[i])
+
+    def pair(i, at):
+        return remote(
+            (tok, cot)[i], whole.at[i, :, at], pair_sem.at[0, i], pair_sem.at[1, i], partner
+        )
+
+    for i in range(2):
+        pair(i, mine).start()
+        own_whole(i).start()
 
     def member(step):
         to = (fast + step) % inner
@@ -132,7 +153,7 @@
             device,
         ).start()
     own_cut = pltpu.make_async_copy(
-        cut.at[:, fast], cut_all.at[:, fast, :, cut_mine], own_sem.at[1]
+        cut.at[:, fast], cut_all.at[:, fast, :, cut_mine], own_sem.at[2]
     )
     own_cut.start()
     remote(
@@ -143,23 +164,37 @@
         partner,
     ).start()
 
-    own_slot = pltpu.make_async_copy(packed.at[:, me], got.at[:, me, :, mine], own_sem.at[2])
-    own_slot.start()
-    remote(
-        packed.at[:, me], got.at[:, me, :, mine], fwd_out_sem.at[me], fwd_in_sem.at[me], partner
-    ).start()
-
-    def send_slots(s):
-        to = lax.rem(me + s, groups)
-        remote(
-            packed.at[:, to], got.at[:, me, :, mine], out_sem.at[to], in_sem.at[me], (to, half)
-        ).start()
-
-    middle = groups // 2
-    loop(1, middle, send_slots)
-
-    own_whole.wait()
-    remote(both, whole.at[:, :, theirs], pair_sem.at[0], pair_sem.at[1], partner).wait()
+    def out_copy(i, to, frm, device):
+        return remote(
+            packed[i].at[to],
+            got[i].at[frm, :, mine],
+            out_sem.at[i, to],
+            in_sem.at[i, frm],
+            device,
+        )
+
+    def forward_copy(i, frm, at):
+        here = got[i].at[frm, :, at]
+        return remote(here, here, fwd_out_sem.at[i, frm], fwd_in_sem.at[i, frm], partner)
+
+    def own_slot(i):
+        return pltpu.make_async_copy(
+            packed[i].at[me], got[i].at[me, :, mine], own_sem.at[3 + i]
+        )
+
+    def over(di, first, body):
+        loop(first, outer, lambda do: body(do, di))
+
+    def send_slots(do, di):
+        to = lax.rem(slow + do, outer) * inner + lax.rem(fast + di, inner)
+        for i in range(2):
+            out_copy(i, to, me, (to, half)).start()
+
+    over(0, 1, send_slots)
+
+    for i in range(2):
+        own_whole(i).wait()
+        pair(i, theirs).wait()
 
     rows = whole[0]
     mix_gate = dot_nn(rows, sgate[...])
@@ -178,7 +213,7 @@
             mixed.at[fast], mixed.at[fast], mixed_sem.at[0, to], mixed_sem.at[1, fast], device
         ).start()
 
-    loop(middle, groups, send_slots)
+    over(1, 1, send_slots)
 
     for piece in range(2):
         at = pl.ds(piece * cols, cols)
@@ -217,7 +252,6 @@
     depth = inner * cut.shape[2]
     wide = 2 * cut_cols
     every = mixed[...].reshape(depth, 3 * hid)
-    block = part.shape[1]
     part[:, :, 0 : 2 * hid] = (
         dot_tn(cut_all[0].reshape(depth, wide), every[:, 0 : 2 * hid])
         .astype(BF16)
@@ -229,117 +263,178 @@
         .reshape(outer, block, hid)
     )
 
-    def send_part(s):
-        to = lax.rem(slow + s, outer)
+    def exchange(stride, first):
+        bit = (slow // stride) % 2
+        low = slow % stride
+        keep = low + bit * stride
+        give = low + (1 - bit) * stride
+        device = ((slow + stride - 2 * bit * stride) * inner + fast, half)
+        count = outer // (2 * stride)
+
+        def copy(n):
+            return remote(
+                part.at[give + 2 * stride * n],
+                part_in.at[first + n],
+                part_sem.at[0, first + n],
+                part_sem.at[1, first + n],
+                device,
+            )
+
+        def start():
+            loop(0, count, lambda n: copy(n).start())
+
+        def finish():
+            loop(0, count, lambda n: copy(n).wait())
+
+        def merged(n):
+            return part[keep + 2 * stride * n].astype(F32) + part_in[first + n].astype(F32)
+
+        def fold():
+            def one(n):
+                part[keep + 2 * stride * n] = merged(n).astype(BF16)
+
+            loop(0, count, one)
+
+        return start, finish, merged, fold, count
+
+    stride, first = 1, 0
+    rest = [(di, 1) for di in range(2, inner)] + [(di, 0) for di in range(1, inner)]
+    while stride < outer:
+        start, finish, merged, fold, count = exchange(stride, first)
+        start()
+        if stride * 2 >= outer:
+            for di, do in rest:
+                loop(do, outer if do else 1, lambda do, di=di: send_slots(do, di))
+        elif rest and rest[0][1]:
+            over(rest[0][0], 1, send_slots)
+            rest = rest[1:]
+        if stride * 2 < outer:
+            finish()
+            fold()
+        first += count
+        stride *= 2
+
+    def forward(do, di):
+        frm = lax.rem(slow + outer - do, outer) * inner + lax.rem(fast + inner - di, inner)
+        for i in range(2):
+            out_copy(i, frm, frm, partner).wait_recv()
+            forward_copy(i, frm, mine).start()
+
+    for i in range(2):
+        own_slot(i).start()
         remote(
-            part.at[to],
-            part_in.at[slow],
-            part_sem.at[0, to],
-            part_sem.at[1, slow],
-            (to * inner + fast, half),
+            packed[i].at[me],
+            got[i].at[me, :, mine],
+            fwd_out_sem.at[i, me],
+            fwd_in_sem.at[i, me],
+            partner,
         ).start()
-
-    loop(1, outer, send_part)
-
-    def forward(s):
-        frm = lax.rem(me + groups - s, groups)
-        here = got.at[:, frm, :, mine]
-        remote(packed.at[:, frm], here, out_sem.at[frm], in_sem.at[frm], partner).wait_recv()
-        remote(here, here, fwd_out_sem.at[frm], fwd_in_sem.at[frm], partner).start()
-
-    loop(1, groups, forward)
-
-    total = part[slow].astype(F32)
+    over(0, 1, forward)
+    over(1, 1, forward)
+    over(2, 1, forward)
+
+    finish()
+    total = merged(0)
     grad_gate[...] = total[:, 0:hid]
     grad_up[...] = total[:, hid : 2 * hid]
     grad_down[...] = total[:, 2 * hid : 3 * hid]
 
-    def take_part(s):
-        frm = lax.rem(slow + outer - s, outer)
-        remote(
-            part.at[frm], part_in.at[frm], part_sem.at[0, frm], part_sem.at[1, frm], partner
-        ).wait()
-        term = part_in[frm].astype(F32)
-        grad_gate[...] += term[:, 0:hid]
-        grad_up[...] += term[:, hid : 2 * hid]
-        grad_down[...] += term[:, 2 * hid : 3 * hid]
-
-    loop(1, outer, take_part)
-
-    own_slot.wait()
-
-    def finish(s):
+    for di in range(1, inner):
+        loop(0, 1, lambda do, di=di: forward(do, di))
+    for di in range(3, inner):
+        over(di, 1, forward)
+
+    def drain(s):
         frm = lax.rem(me + groups - s, groups)
-        here = got.at[:, frm, :, mine]
-        there = got.at[:, frm, :, theirs]
-        remote(here, there, fwd_out_sem.at[frm], fwd_in_sem.at[frm], partner).wait()
-
-    loop(0, groups, finish)
+        for i in range(2):
+            forward_copy(i, frm, mine).wait_send()
+            forward_copy(i, frm, theirs).wait_recv()
+
+    loop(0, groups, drain)
+    for i in range(2):
+        own_slot(i).wait()
 
     def sent(s):
         to = lax.rem(me + s, groups)
-        here = got.at[:, to, :, mine]
-        remote(packed.at[:, to], here, out_sem.at[to], in_sem.at[to], partner).wait_send()
+        for i in range(2):
+            out_copy(i, to, to, partner).wait_send()
 
     loop(1, groups, sent)
 
 
-def dispatch(groups, inner, both, packed, cut, sgate, sup, sdown):
-    _, token_rows, cols = both.shape
-    per_peer = packed.shape[2]
+def dispatch(groups, inner, tok, cot, packed_rows, packed_cot, sgate, sup, sdown):
+    token_rows, cols = tok.shape
+    per_peer = packed_rows.shape[1]
     width = 2 * cols
     hid = sgate.shape[1]
     outer = groups // inner
     block = width // groups
     vmem = pl.BlockSpec(memory_space=pltpu.VMEM)
+    anyspace = pl.BlockSpec(memory_space=pl.ANY)
+    slots = jax.ShapeDtypeStruct((groups, per_peer, width), BF16)
     grad = jax.ShapeDtypeStruct((block, hid), F32)
     dma = pltpu.SemaphoreType.DMA
     return pl.pallas_call(
         functools.partial(dispatch_kernel, groups, inner),
         out_shape=(
-            jax.ShapeDtypeStruct((2, groups, per_peer, width), BF16),
+            slots,
+            slots,
             jax.ShapeDtypeStruct((token_rows, cols), F32),
             grad,
             grad,
             grad,
         ),
-        in_specs=[vmem] * 6,
-        out_specs=(pl.BlockSpec(memory_space=pl.ANY), vmem, vmem, vmem, vmem),
+        in_specs=[vmem] * 7,
+        out_specs=(anyspace, anyspace, vmem, vmem, vmem, vmem),
         scratch_shapes=[
             pltpu.VMEM((2, token_rows, width), BF16),
+            pltpu.VMEM((2, inner, token_rows, cols // inner), BF16),
             pltpu.VMEM((2, inner, token_rows, width // inner), BF16),
             pltpu.VMEM((inner, token_rows, 3 * hid), BF16),
             pltpu.VMEM((2, token_rows, cols), BF16),
             pltpu.VMEM((token_rows, cols), BF16),
             pltpu.VMEM((outer, block, 3 * hid), BF16),
             pltpu.VMEM((outer, block, 3 * hid), BF16),
+            dma((2, 2)),
             dma((2,)),
-            dma((2,)),
-            dma((3,)),
-            dma((groups,)),
-            dma((groups,)),
-            dma((groups,)),
-            dma((groups,)),
+            dma((5,)),
+            dma((2, groups)),
+            dma((2, groups)),
+            dma((2, groups)),
+            dma((2, groups)),
             dma((4, inner)),
             dma((2, inner)),
             dma((2, outer)),
         ],
         compiler_params=pltpu.CompilerParams(collective_id=0, has_side_effects=True),
         name="dispatch",
-    )(both, packed, cut, sgate, sup, sdown)
-
-
-def home_kernel(groups, terms, home, taken, back, pair_sem, own_sem, out_sem, in_sem):
+    )(tok, cot, packed_rows, packed_cot, sgate, sup, sdown)
+
+
+def home_kernel(groups, terms, lanes, home, taken, back, pair_sem, own_sem, out_sem, in_sem):
     me = lax.axis_index("ep")
     half = lax.axis_index("tp")
     other = 1 - half
     greet(groups, me, half)
-    pair = remote(terms.at[other], taken, pair_sem.at[0], pair_sem.at[1], (me, other))
+    wide, cols = lanes.shape[2], terms.shape[2] // 2
+    mine = pl.ds(pl.multiple_of(half * cols, cols), cols)
+    theirs = pl.ds(pl.multiple_of(other * cols, cols), cols)
+    main, tail = pl.ds(0, cols), pl.ds(cols, wide)
+    partner = (me, other)
+    pair = remote(
+        terms.at[:, :, theirs], taken.at[:, :, main], pair_sem.at[0, 0], pair_sem.at[1, 0], partner
+    )
+    side = remote(lanes, taken.at[:, :, tail], pair_sem.at[0, 1], pair_sem.at[1, 1], partner)
     pair.start()
+    side.start()
     pair.wait()
+    side.wait()
 
     def add(s):
-        back[s] = (terms[half, s].astype(F32) + taken[s].astype(F32)).astype(BF16)
+        back[s, :, main] = (terms[s, :, mine].astype(F32) + taken[s, :, main].astype(F32)).astype(
+            BF16
+        )
+        back[s, :, tail] = (lanes[s].astype(F32) + taken[s, :, tail].astype(F32)).astype(BF16)
 
     loop(0, groups, add)
     own = pltpu.make_async_copy(back.at[me], home.at[me], own_sem)
@@ -359,26 +454,26 @@
     loop(1, groups, take)
 
 
-def send_home(groups, terms):
-    shape = terms.shape[1:]
+def send_home(groups, terms, lanes):
+    shape = (*terms.shape[:2], terms.shape[2] // 2 + lanes.shape[2])
     vmem = pl.BlockSpec(memory_space=pltpu.VMEM)
     dma = pltpu.SemaphoreType.DMA
     return pl.pallas_call(
         functools.partial(home_kernel, groups),
         out_shape=jax.ShapeDtypeStruct(shape, BF16),
-        in_specs=[vmem],
+        in_specs=[vmem, vmem],
         out_specs=pl.BlockSpec(memory_space=pl.ANY),
         scratch_shapes=[
             pltpu.VMEM(shape, BF16),
             pltpu.VMEM(shape, BF16),
-            dma((2,)),
+            dma((2, 2)),
             dma,
             dma((groups,)),
             dma((groups,)),
         ],
         compiler_params=pltpu.CompilerParams(collective_id=1, has_side_effects=True),
         name="home",
-    )(terms)
+    )(terms, lanes)
 
 
 def per_device(
@@ -394,7 +489,6 @@
     shared_down,
 ):
     groups = lax.axis_size("ep")
-    halves = lax.axis_size("tp")
     local_count = gate_proj.shape[0]
     experts = groups * local_count
     token_rows, top = routes.shape
@@ -404,8 +498,6 @@
     slots = experts * capacity
     cols = tokens.shape[1]
     inner = 4
-    outer = groups // inner
-    block = halves * cols // groups
 
     names = routes.T
     named = (names[:, :, None] == jnp.arange(experts, dtype=jnp.int32)).astype(BF16)
@@ -419,15 +511,16 @@
     slot_weight = jnp.sum(jnp.where(hit, route_weights.T[:, None, :], 0.0), axis=(0, 2))
     packed_rows = dot_nn(chosen, tokens).astype(BF16)
     packed_cot = (slot_weight[:, None] * dot_nn(chosen, cotangent)).astype(BF16)
-    packed = jnp.stack([packed_rows, packed_cot]).reshape(2, groups, per_peer, cols)
-    both = jnp.stack([tokens, cotangent])
-    cut = (
-        both.reshape(2, token_rows, outer // halves, inner, block)
-        .transpose(0, 3, 1, 2, 4)
-        .reshape(2, inner, token_rows, cols // inner)
-    )
-    got, mix_sum, sharedgate_grad, sharedup_grad, shareddown_grad = dispatch(
-        groups, inner, both, packed, cut, shared_gate, shared_up, shared_down
+    got_rows, got_cot, mix_sum, sharedgate_grad, sharedup_grad, shareddown_grad = dispatch(
+        groups,
+        inner,
+        tokens,
+        cotangent,
+        packed_rows.reshape(groups, per_peer, cols),
+        packed_cot.reshape(groups, per_peer, cols),
+        shared_gate,
+        shared_up,
+        shared_down,
     )
 
     def by_expert(layout):
@@ -440,8 +533,8 @@
             groups, per_peer, -1
         )
 
-    slot_rows = by_expert(got[0])
-    slot_cot = by_expert(got[1])
+    slot_rows = by_expert(got_rows)
+    slot_cot = by_expert(got_cot)
     gate_pre = jnp.einsum("erd,edf->erf", slot_rows, gate_proj, preferred_element_type=F32)
     up_pre = jnp.einsum("erd,edf->erf", slot_rows, up_proj, preferred_element_type=F32)
     gate_act, gate_slope = silu_parts(gate_pre)
@@ -457,13 +550,7 @@
     )
     sent_part = by_peer(input_part.astype(BF16))
     lanes = jnp.broadcast_to(by_peer(product.astype(BF16)), (groups, per_peer, 128))
-    terms = jnp.stack(
-        [
-            jnp.concatenate([sent_part[:, :, h * cols : (h + 1) * cols], lanes], axis=2)
-            for h in range(halves)
-        ]
-    )
-    home = send_home(groups, terms).reshape(slots, cols + 128)
+    home = send_home(groups, sent_part, lanes).reshape(slots, cols + 128)
 
     down_grad = jnp.einsum("erf,erd->efd", hidden_low, slot_cot, preferred_element_type=F32)
     gate_grad = jnp.einsum("erd,erf->edf", slot_rows, gate_delta, preferred_element_type=F32)

time: 122 us -> 125 us (1.025); the launches traced: 122 us -> 124 us
  Pallas kernels: 91 us -> 96.4 us
  other arithmetic: 8.25 us -> 3.82 us
  matrix products: 13.9 us -> 18.2 us
  local copies, waits for them, and re-layouts: 8.01 us -> 4.48 us
    another operation x4 -> x0, other arithmetic: 3.69 us -> none  [the longest x2 1.56 us: per_device(): jnp.stack([jnp.concatenate([sent_part[:, :, h * cols:(h + 1) * cols], lan...]
    pallas_call x1, Pallas kernels: 61.1 us -> 64.6 us  [dispatch(): pl.pallas_call(functools.partial(dispatch_kernel, groups, inner), out_sha...]
    slice x2 -> x0, local copies, waits for them, and re-layouts: 2.47 us -> none  [the longest x1 2.35 us: per_device(): slot_rows = by_expert(got[0])]
    pallas_call x1, Pallas kernels: 29.9 us -> 31.8 us  [send_home(): pl.pallas_call(functools.partial(home_kernel, groups), out_shape=jax.Shap...]
    dot_general x3, matrix products: 2.77 us -> 4.53 us  [dot_nn(): lax.dot_general(left, right, (((1,), (0,)), ((), ())), preferred_element_...]
    dot_general x1, matrix products: 0.95 us -> 2.31 us  [per_device(): jnp.einsum('erd,edf->erf', slot_rows, gate_proj, preferred_element_type=F32)]
where the time goes in v2:
time: 125 us; the launch traced here: 124 us
  Pallas kernels  96.4 us (77%)
  matrix products  18.2 us (15%)
  local copies, waits for them, and re-layouts  4.48 us (4%)
  other arithmetic  3.82 us (3%)
    pallas_call x1, Pallas kernels, dispatch(): pl.pallas_call(functools.partial(dispatch_kernel, groups, inner), out_sha...  64.6 us
    pallas_call x1, Pallas kernels, send_home(): pl.pallas_call(functools.partial(home_kernel, groups), out_shape=jax.Shap...  31.8 us
    dot_general x3, matrix products, dot_nn(): lax.dot_general(left, right, (((1,), (0,)), ((), ())), preferred_element_...  4.53 us
    unnamed x24, local copies, waits for them, and re-layouts  2.73 us

profile of v2, /device:TPU:12, one launch (start us, length us, event | category | flops | bytes accessed | tf_op | source)
XLA Modules:
  0.0 123.7 jit_solution(4696848803234694123)
XLA Ops:
  0.6 0.8 fusion.19
  1.6 0.7 multiply_reduce_fusion.1
  2.3 0.7 convert_add_fusion
  3.0 0.8 select_reduce_fusion.1
  3.9 2.2 %multiply_convert_fusion = bf16[384,1024]{1,0:T(8,128)(2,1)} fusion(bf16[128,1024]{1,0:T(8,128)(2,1)} %cot.1, f32[384]{0:T(512)S(1)} %select_reduce_fusion.1, pred[2,384,128]{2,1,0:T(32,128)(4,1)S(1)} %iota_compare_fusion), kind=kOutput, calls=%fused_computation.7 | convolution fusion | flops 101498880 | bytes 1148416 | tf_op jit(solution)/shard_map/dot_general | solution.py:32
  6.1 2.2 %convolution_convert_fusion.3 = bf16[384,1024]{1,0:T(8,128)(2,1)} fusion(bf16[128,1024]{1,0:T(8,128)(2,1)} %tok.1, pred[2,384,128]{2,1,0:T(32,128)(4,1)S(1)} %iota_compare_fusion), kind=kOutput, calls=%fused_computation.8 | convolution fusion | flops 101105664 | bytes 1146880 | tf_op jit(solution)/shard_map/dot_general | solution.py:32
  8.3 64.6 %dispatch.1 = (bf16[16,24,2048]{2,1,0:T(8,128)(2,1)}, bf16[16,24,2048]{2,1,0:T(8,128)(2,1)}, f32[128,1024]{1,0:T(8,128)}, f32[128,256]{1,0:T(8,128)}, f32[128,256]{1,0:T(8,128)}, /*index=5*/f32[128,256]{1,0:T(8,128)}) custom-call(bf16[128,1024]{1,0:T(8,128)(2,1)} %tok.1, bf16[128,1024]{1,0:T(8,128)(2,1)} %cot.1, bf16[16,24,1024]{2,1,0:T(8,128)(2,1)} %bitcast.60, ...), custom_call_target="tpu_custom_call" | custom-call | tf_op jit(solution)/shard_map/dispatch/pallas_call | solution.py:377
  72.9 2.3 %fusion.6 = f32[384,256]{0,1:T(8,128)S(1)} fusion(bf16[384,2048]{1,0:T(8,128)(2,1)} %bitcast.52, bf16[1,2048,256]{2,1,0:T(8,128)(2,1)S(1)} %copy-done), kind=kOutput, calls=%fused_computation.13 | convolution fusion | flops 402653184 | bytes 3014656 | tf_op jit(solution)/shard_map/erd,edf->erf/dot_general | solution.py:538
  75.2 0.8 fusion.9
  76.0 0.6 copy-done.8
  76.6 1.7 %fusion.2 = bf16[1,256,2048]{2,1,0:T(8,128)(2,1)} fusion(bf16[384,2048]{1,0:T(8,128)(2,1)S(1)} %bitcast.64, f32[384,256]{0,1:T(8,128)S(1)} %fusion.9, f32[384,256]{0,1:T(8,128)S(1)} %fusion.6), kind=kOutput, calls=%fused_computation.6 | convolution fusion | flops 403767296 | bytes 3407872 | tf_op jit(solution)/shard_map/erf,erd->efd/dot_general | solution.py:555
  78.3 0.8 multiply_reduce_fusion
  79.1 1.7 %fusion = bf16[1,2048,256]{2,1,0:T(8,128)(2,1)} fusion(bf16[384,2048]{1,0:T(8,128)(2,1)S(1)} %bitcast.54, bf16[384,256]{0,1:T(8,128)(2,1)S(1)} %get-tuple-element.21), kind=kOutput, calls=%fused_computation.4 | convolution fusion | flops 403177472 | bytes 2818048 | tf_op jit(solution)/shard_map/erd,erf->edf/dot_general | solution.py:556
  80.8 1.7 %fusion.1 = bf16[1,2048,256]{2,1,0:T(8,128)(2,1)} fusion(bf16[384,2048]{1,0:T(8,128)(2,1)S(1)} %bitcast.55, bf16[384,256]{0,1:T(8,128)(2,1)S(1)} %get-tuple-element.22), kind=kOutput, calls=%fused_computation.5 | convolution fusion | flops 403177472 | bytes 2818048 | tf_op jit(solution)/shard_map/erd,erf->edf/dot_general | solution.py:557
  82.6 0.6 fusion.4
  83.2 1.8 %add_convert_fusion = bf16[384,2048]{1,0:T(8,128)(2,1)} fusion(f32[384,2048]{1,0:T(8,128)S(1)} %fusion.4, bf16[384,256]{0,1:T(8,128)(2,1)S(1)} %get-tuple-element.22, bf16[1,2048,256]{2,1,0:T(8,128)(2,1)S(1)} %copy-done.2), kind=kOutput, calls=%fused_computation | convolution fusion | flops 404226048 | bytes 5963776 | tf_op jit(solution)/shard_map/erf,edf->erd/dot_general | solution.py:548
  85.1 0.8 broadcast_in_dim.22.lanes
  85.9 31.8 %home.1 = bf16[16,24,1152]{2,1,0:T(8,128)(2,1)} custom-call(bf16[16,24,2048]{2,1,0:T(8,128)(2,1)} %bitcast.56, bf16[16,24,128]{2,1,0:T(8,128)(2,1)} %broadcast_in_dim.22.lanes), custom_call_target="tpu_custom_call" | custom-call | tf_op jit(solution)/shard_map/home/pallas_call | solution.py:461
  117.7 2.3 %fusion.3 = bf16[128,1024]{1,0:T(8,128)(2,1)} fusion(f32[128,1024]{1,0:T(8,128)S(1)} %copy-done.3, bf16[384,1152]{1,0:T(8,128)(2,1)} %bitcast.57, pred[2,384,128]{2,1,0:T(32,128)(4,1)S(1)} %iota_compare_fusion), kind=kOutput, calls=%fused_computation.10 | convolution fusion | flops 100974592 | bytes 1671168 | tf_op jit(solution)/shard_map/dot_general | solution.py:40
  120.0 0.9 slice.29
  121.2 0.6 bitcast_divide_fusion
  121.7 0.7 copy.27
  122.4 0.7 copy.28
  123.1 0.7 copy.29
  (25 shorter events, 0.6 us)
Async XLA Ops:
  0.6 72.2 %copy-start = (bf16[1,2048,256]{2,1,0:T(8,128)(2,1)S(1)}, bf16[1,2048,256]{2,1,0:T(8,128)(2,1)}, u32[]{:S(2)}) copy-start(bf16[1,2048,256]{2,1,0:T(8,128)(2,1)} %param.14) | copy-start | bytes 3145732
  72.8 2.4 %copy-start.1 = (bf16[16,24,2048]{2,1,0:T(8,128)(2,1)S(1)}, bf16[16,24,2048]{2,1,0:T(8,128)(2,1)}, u32[]{:S(2)}) copy-start(bf16[16,24,2048]{2,1,0:T(8,128)(2,1)} %get-tuple-element.16) | copy-start | bytes 4718596
  72.8 2.4 %copy-start.2 = (bf16[1,2048,256]{2,1,0:T(8,128)(2,1)S(1)}, bf16[1,2048,256]{2,1,0:T(8,128)(2,1)}, u32[]{:S(2)}) copy-start(bf16[1,2048,256]{2,1,0:T(8,128)(2,1)} %param.15) | copy-start | bytes 3145732
  75.2 1.4 %copy-start.8 = (bf16[16,24,2048]{2,1,0:T(8,128)(2,1)S(1)}, bf16[16,24,2048]{2,1,0:T(8,128)(2,1)}, u32[]{:S(2)}) copy-start(bf16[16,24,2048]{2,1,0:T(8,128)(2,1)} %get-tuple-element.15) | copy-start | bytes 4718596
  76.6 1.7 %copy-start.9 = (bf16[1,256,2048]{2,1,0:T(8,128)(2,1)S(1)}, bf16[1,256,2048]{2,1,0:T(8,128)(2,1)}, u32[]{:S(2)}) copy-start(bf16[1,256,2048]{2,1,0:T(8,128)(2,1)} %param.16) | copy-start | bytes 3145732
  85.0 32.7 %copy-start.3 = (f32[128,1024]{1,0:T(8,128)S(1)}, f32[128,1024]{1,0:T(8,128)}, u32[]{:S(2)}) copy-start(f32[128,1024]{1,0:T(8,128)} %get-tuple-element.14) | copy-start | bytes 1572868
  117.7 3.5 %copy-start.7 = (f32[128,2]{0,1:T(2,128)S(1)}, f32[128,2]{0,1:T(2,128)}, u32[]{:S(2)}) copy-start(f32[128,2]{0,1:T(2,128)} %param.13) | copy-start | bytes 3076
  117.7 4.1 %copy-start.6 = (f32[128,256]{1,0:T(8,128)S(1)}, f32[128,256]{1,0:T(8,128)}, u32[]{:S(2)}) copy-start(f32[128,256]{1,0:T(8,128)} %get-tuple-element.36) | copy-start | bytes 393220
  117.7 4.7 %copy-start.5 = (f32[128,256]{1,0:T(8,128)S(1)}, f32[128,256]{1,0:T(8,128)}, u32[]{:S(2)}) copy-start(f32[128,256]{1,0:T(8,128)} %get-tuple-element.37) | copy-start | bytes 393220
  117.7 5.4 %copy-start.4 = (f32[128,256]{1,0:T(8,128)S(1)}, f32[128,256]{1,0:T(8,128)}, u32[]{:S(2)}) copy-start(f32[128,256]{1,0:T(8,128)} %get-tuple-element.38) | copy-start | bytes 393220
